TPU v7x, 32 devices: a whole 2x2x4 slice. The times are simulated.
32 devices in a mesh: sp: 8 (over z, x), tp: 4 (over y, core).
Axes of the slice: x: 2, y: 2, z: 4, core: 2. Of those that a mesh axis runs over, the one named last changes fastest.
Arguments:
- resid: bfloat16 [1024, 2048], P('sp'), may hold values from -8 to 8
- a_val: bfloat16 [1024, 1024], P('sp', 'tp'), may hold values from -8 to 8
- a_gate: bfloat16 [1024, 1024], P('sp', 'tp'), may hold values from -6 to 6
- conv_kernel: bfloat16 [31, 1024], P(None, 'tp'), may hold values from -1 to 1
- conv_bias: float32 [1024], P('tp'), may hold values from -3 to 3
- ln_gain: float32 [1024], P('tp'), may hold values from 0.1 to 1.9
- ln_bias: float32 [1024], P('tp'), may hold values from -3 to 3
- w_out: bfloat16 [1024, 2048], P('tp'), may hold values from -0.1875 to 0.1875
- ffn_gain: float32 [2048], replicated, may hold values from 0.1 to 1.9
- routes: int32 [1024, 4], P('sp'), may hold values from 0 to 7, all different within a row; in each aligned block of 128 rows (0 to 127, 128 to 255, ...) at most 128 rows name the same one
- route_weights: float32 [1024, 4], P('sp'), may hold values from 0.15 to 1.2
- exp_gate: bfloat16 [8, 2048, 4096], P('sp', None, 'tp'), may hold values from -0.125 to 0.125
- exp_up: bfloat16 [8, 2048, 4096], P('sp', None, 'tp'), may hold values from -0.125 to 0.125
- exp_down: bfloat16 [8, 4096, 2048], P('sp', None, 'tp'), may hold values from -0.09375 to 0.09375
- sh_gate: bfloat16 [2048, 512], P(None, 'tp'), may hold values from -0.125 to 0.125
- sh_up: bfloat16 [2048, 512], P(None, 'tp'), may hold values from -0.125 to 0.125
- sh_down: bfloat16 [512, 2048], P(None, 'tp'), may hold values from -0.25 to 0.25
Outputs:
- result: bfloat16 [1024, 2048], P('sp', 'tp')
Inputs may be any that keep to these rules, and one draw needn't show every extreme that they name: `routes`: among the 128 rows of one index of sp, each expert is named at most 128 times, a bound that some block reaches; a row names 4 different experts.
All inputs are finite; a program needn't handle non-finite values.
Results may differ from a plain program's by a relative error of at most 0.007.
Values may be sent and summed in bfloat16 or wider, within the bound.
A program may use at most 64 MiB of HBM per device.

v0:
```python
import jax
import jax.numpy as jnp
from jax import lax
from jax.sharding import PartitionSpec as P

LN_EPS = 1e-05
RMS_EPS = 1e-06


def shifted(value, axis, by):
    size = lax.axis_size(axis)
    pairs = [(i, i + by) for i in range(size) if 0 <= i + by < size]
    return lax.ppermute(value, axis, pairs)


def body(
    resid,
    a_val,
    a_gate,
    conv_kernel,
    conv_bias,
    ln_gain,
    ln_bias,
    w_out,
    ffn_gain,
    routes,
    route_weights,
    exp_gate,
    exp_up,
    exp_down,
    sh_gate,
    sh_up,
    sh_down,
):
    tp_count = lax.axis_size("tp")
    tp_place = lax.axis_index("tp")
    sp_count = lax.axis_size("sp")
    tok_rows = resid.shape[0]
    model_width = resid.shape[1]
    col_width = model_width // tp_count
    col_start = tp_place * col_width
    conv_span = conv_kernel.shape[0]
    channels_all = a_val.shape[1] * tp_count
    gated_in = (a_val.astype(jnp.float32) * jax.nn.sigmoid(a_gate.astype(jnp.float32))).astype(
        jnp.bfloat16
    )
    before = shifted(gated_in[tok_rows - (conv_span - 1) :], "sp", 1)
    padded = jnp.concatenate([before, gated_in], axis=0).astype(jnp.float32)
    kernel = conv_kernel.astype(jnp.float32)

    def add_tap(offset, running):
        window_rows = lax.dynamic_slice_in_dim(padded, offset, tok_rows, 0)
        return running + lax.dynamic_slice_in_dim(kernel, offset, 1, 0) * window_rows

    start_sum = jnp.broadcast_to(conv_bias[None, :], gated_in.shape)
    conv_out = lax.fori_loop(0, conv_span, add_tap, start_sum)
    row_sums = lax.psum((jnp.sum(conv_out, axis=1), jnp.sum(conv_out * conv_out, axis=1)), "tp")
    channel_mean = row_sums[0] / channels_all
    channel_var = row_sums[1] / channels_all - channel_mean * channel_mean
    scaled = (conv_out - channel_mean[:, None]) * lax.rsqrt(
        channel_var[:, None] + LN_EPS
    ) * ln_gain[None, :] + ln_bias[None, :]
    mixed_out = jax.nn.silu(scaled).astype(jnp.bfloat16)
    partial_proj = jnp.dot(mixed_out, w_out, preferred_element_type=jnp.float32)
    projected = lax.psum(partial_proj, "tp")
    middle = (resid.astype(jnp.float32) + projected).astype(jnp.bfloat16)
    middle_f = middle.astype(jnp.float32)
    inverse = lax.rsqrt(jnp.mean(middle_f * middle_f, axis=1, keepdims=True) + RMS_EPS)
    normed = (middle_f * inverse * ffn_gain[None, :]).astype(jnp.bfloat16)
    middle_cols = lax.dynamic_slice_in_dim(middle, col_start, col_width, 1)
    shared_gate = jnp.dot(normed, sh_gate, preferred_element_type=jnp.float32)
    shared_up = jnp.dot(normed, sh_up, preferred_element_type=jnp.float32)
    shared_hidden = (jax.nn.silu(shared_gate) * shared_up).astype(jnp.bfloat16)
    weight_rows = sh_down
    shared = jnp.dot(
        lax.all_gather(shared_hidden, "tp", axis=1, tiled=True),
        weight_rows,
        preferred_element_type=jnp.float32,
    )
    top_count = routes.shape[1]
    local_experts = exp_gate.shape[0]
    experts_all = local_experts * sp_count
    capacity = max(2 * tok_rows * top_count // experts_all, tp_count)
    pair_count = tok_rows * top_count
    chosen = routes.reshape(pair_count)
    one_hot = (chosen[:, None] == jnp.arange(experts_all, dtype=jnp.int32)[None, :]).astype(
        jnp.int32
    )
    earlier = jnp.cumsum(one_hot, axis=0) - one_hot
    place_in = jnp.sum(earlier * one_hot, axis=1)
    slot_of = chosen * capacity + place_in
    owner_ids = (
        jnp.zeros((experts_all * capacity,), jnp.int32)
        .at[slot_of]
        .set(jnp.arange(pair_count, dtype=jnp.int32) + 1)
    )
    owner_grid = owner_ids.reshape(sp_count, local_experts, capacity)
    part_slots = capacity // tp_count
    own_owners = lax.dynamic_slice_in_dim(owner_grid, tp_place * part_slots, part_slots, 2)
    source_row = jnp.maximum(own_owners - 1, 0) // top_count
    taken = normed[source_row.reshape(-1)].reshape(own_owners.shape + (model_width,))
    landed = lax.all_to_all(
        jnp.where((own_owners > 0)[..., None], taken, jnp.zeros((), jnp.bfloat16)),
        "sp",
        split_axis=0,
        concat_axis=0,
        tiled=True,
    )
    arrived = lax.all_gather(landed, "tp", axis=2, tiled=True)
    gate_part = jnp.einsum("sxcd,xdf->sxcf", arrived, exp_gate, preferred_element_type=jnp.float32)
    up_part = jnp.einsum("sxcd,xdf->sxcf", arrived, exp_up, preferred_element_type=jnp.float32)
    expert_hidden = (jax.nn.silu(gate_part) * up_part).astype(jnp.bfloat16)
    weight_rows = exp_down
    expert_sum = jnp.einsum(
        "sxcf,xfd->sxcd",
        lax.all_gather(expert_hidden, "tp", axis=3, tiled=True),
        weight_rows,
        preferred_element_type=jnp.float32,
    )
    expert_out = expert_sum.astype(jnp.bfloat16)
    returned = lax.all_to_all(expert_out, "sp", split_axis=0, concat_axis=0, tiled=True)
    flat_out = returned.reshape(experts_all * capacity, col_width)
    picked = flat_out[slot_of].astype(jnp.float32).reshape(tok_rows, top_count, col_width)
    routed = jnp.sum(picked * route_weights[:, :, None], axis=1)
    return (middle_cols.astype(jnp.float32) + shared + routed).astype(jnp.bfloat16)


def solution(mesh):
    in_specs = (
        P("sp", None),
        P("sp", "tp"),
        P("sp", "tp"),
        P(None, "tp"),
        P("tp"),
        P("tp"),
        P("tp"),
        P("tp", None),
        P(),
        P("sp", None),
        P("sp", None),
        P("sp", None, "tp"),
        P("sp", None, "tp"),
        P("sp", None, "tp"),
        P(None, "tp"),
        P(None, "tp"),
        P(None, "tp"),
    )
    out_specs = P("sp", "tp")
    return jax.shard_map(body, mesh=mesh, in_specs=in_specs, out_specs=out_specs, check_vma=False)
```

profile of v0, /device:TPU:0, one launch (start us, length us, event | category | flops | bytes accessed | tf_op | source)
XLA Modules:
  0.0 262.0 jit_solution(12313480295030517520)
XLA Ops:
  6.5 1.0 multiply_convert_fusion.1
  7.6 4.9 %collective-permute-start = (bf16[30,256]{1,0:T(8,128)(2,1)S(1)}, bf16[30,256]{1,0:T(8,128)(2,1)S(1)}, u32[]{:S(2)}, u32[]{:S(2)}) collective-permute-start(bf16[30,256]{1,0:T(8,128)(2,1)S(1)} %slice.16), channel_id=1, source_target_pairs={{0,4},{4,8},{8,12},{12,16},{16,20},{20,24},{24,28},{1,5},{5,9},{9,... | collective-permute-start | bytes 46088 | tf_op jit(solution)/shard_map/ppermute | solution.py:13
  12.5 0.7 broadcast_multiply_fusion
  13.2 0.8 copy.24
  13.9 0.1 eq.29
  14.1 0.1 eq.25
  14.2 0.0 copy-start.2
  14.2 0.1 copy.23
  14.3 0.1 mul.137
  14.4 1.1 reduce-window.6
  15.6 0.2 slice_reduce_fusion
  15.8 0.1 fusion.40
  15.9 0.7 convert_element_type.69
  16.7 2.4 scatter_custom_fusion
  19.1 0.7 broadcast_in_dim.14
  19.8 2.4 while.13
  22.3 0.1 fusion.46
  22.4 6.3 %all-reduce = (f32[128]{0:T(128)S(1)}, f32[128]{0:T(128)S(1)}) all-reduce(f32[128]{0:T(128)S(1)} %get-tuple-element.86, f32[128]{0:T(128)S(1)} %get-tuple-element.85), channel_id=1, replica_groups=mesh['sp'=8,'tp'=4] {'tp'}, use_global_device_ids=true, to_apply=%region_5.0 | all-reduce | flops 256 | bytes 2048 | tf_op jit(solution)/shard_map/psum | solution.py:57
  28.7 2.1 fusion.33
  30.8 0.0 all-reduce.3.cloned.1.call-update
  30.9 0.0 all-gather.3.cloned.1.call-start
  30.9 0.1 add_select_fusion
  31.0 0.1 reshape.144
  31.1 0.1 compare_bitcast_fusion
  31.2 36.0 %all-reduce.3.cloned.1.call-done = f32[128,2048]{1,0:T(8,128)} async-done(((f32[128,2048]{1,0:T(8,128)}), f32[128,2048]{1,0:T(8,128)}) %all-reduce.3.cloned.1.call-update) | async-done | bytes 1048592 | tf_op jit(solution)/shard_map/psum | solution.py:65
  67.2 1.5 fusion.30
  68.7 0.2 fusion.32
  68.9 1.4 gather_fusion
  70.2 0.1 broadcast_select_fusion
  70.4 30.6 %all_to_all.10 = bf16[8,1,32,2048]{3,2,1,0:T(8,128)(2,1)} all-to-all(bf16[8,1,32,2048]{3,2,1,0:T(8,128)(2,1)S(1)} %broadcast_select_fusion), channel_id=1, replica_groups=mesh['sp'=8,'tp'=4] {'sp'}, dimensions={0} | all-to-all | bytes 2097152 | tf_op jit(solution)/shard_map/all_to_all | solution.py:102
  101.0 0.0 all-gather.3.cloned.1.call-update
  101.1 0.0 all-gather.5.cloned.1.call-start
  101.1 33.4 %all-gather.3.cloned.1.call-done = bf16[8,1,128,2048]{3,2,0,1:T(8,128)(2,1)} async-done(((bf16[8,1,32,2048]{3,2,0,1:T(8,128)(2,1)}), bf16[8,1,128,2048]{3,2,0,1:T(8,128)(2,1)}) %all-gather.3.cloned.1.call-update) | async-done | bytes 4194320 | tf_op jit(solution)/shard_map/all_gather | solution.py:109
  134.6 7.7 %fusion.4 = f32[8,128,1024]{2,1,0:T(8,128)S(1)} fusion(bf16[1,2048,1024]{2,1,0:T(8,128)(2,1)} %param.31, bf16[8,1,128,2048]{3,2,0,1:T(8,128)(2,1)} %all-gather.3.cloned.1.call-done), kind=kOutput, calls=%fused_computation.10 | convolution fusion | flops 4294967296 | bytes 12582912 | tf_op jit(solution)/shard_map/sxcd,xdf->sxcf/dot_general | solution.py:111
  142.2 6.4 %fusion.2 = bf16[8,1,128,1024]{3,2,0,1:T(8,128)(2,1)} fusion(f32[8,128,1024]{2,1,0:T(8,128)S(1)} %fusion.4, bf16[1,2048,1024]{2,1,0:T(8,128)(2,1)S(1)} %copy-done.4, bf16[8,1,128,2048]{3,2,0,1:T(8,128)(2,1)S(1)} %copy-done.5), kind=kOutput, calls=%fused_computation.8 | convolution fusion | flops 4301258752 | bytes 14680064 | tf_op jit(solution)/shard_map/sxcd,xdf->sxcf/dot_general | solution.py:110
  148.6 0.0 all-gather.5.cloned.1.call-update
  148.6 58.4 %all-gather.5.cloned.1.call-done = bf16[8,1,128,4096]{3,2,0,1:T(8,128)(2,1)} async-done(((bf16[8,1,128,1024]{3,2,0,1:T(8,128)(2,1)}), bf16[8,1,128,4096]{3,2,0,1:T(8,128)(2,1)}) %all-gather.5.cloned.1.call-update) | async-done | bytes 8388624 | tf_op jit(solution)/shard_map/all_gather | solution.py:116
  207.0 10.1 %fusion.22 = bf16[8,1,128,512]{3,2,1,0:T(8,128)(2,1)} fusion(bf16[1,4096,512]{2,1,0:T(8,128)(2,1)} %param.32, bf16[8,1,128,4096]{3,2,0,1:T(8,128)(2,1)} %all-gather.5.cloned.1.call-done), kind=kOutput, calls=%fused_computation.22 | convolution fusion | flops 4295491584 | bytes 13631488 | tf_op jit(solution)/shard_map/sxcf,xfd->sxcd/dot_general | solution.py:114
  217.2 5.5 %all-to-all-start.1 = ((bf16[8,1,128,512]{3,2,1,0:T(8,128)(2,1)}), bf16[8,1,128,512]{3,2,1,0:T(8,128)(2,1)S(1)}, u32[]{:S(2)}, u32[]{:S(2)}) async-start(bf16[8,1,128,512]{3,2,1,0:T(8,128)(2,1)} %fusion.22), calls=%async_computation.1 | async-start | bytes 2097152 | tf_op jit(solution)/shard_map/all_to_all | solution.py:121
  222.7 0.1 copy.29
  222.8 1.3 fusion.47
  224.1 1.3 fusion.29
  225.5 5.4 %all_gather.9 = bf16[128,512]{1,0:T(8,128)(2,1)S(1)} all-gather(bf16[128,128]{1,0:T(8,128)(2,1)S(1)} %fusion.29), channel_id=1, replica_groups=mesh['sp'=8,'tp'=4] {'tp'}, dimensions={1}, use_global_device_ids=true | all-gather | bytes 163840 | tf_op jit(solution)/shard_map/all_gather | solution.py:76
  230.9 17.9 %all-to-all-done.1 = bf16[8,1,128,512]{3,2,1,0:T(8,128)(2,1)S(1)} async-done(((bf16[8,1,128,512]{3,2,1,0:T(8,128)(2,1)}), bf16[8,1,128,512]{3,2,1,0:T(8,128)(2,1)S(1)}, u32[]{:S(2)}, u32[]{:S(2)}) %all-to-all-start.1) | async-done | bytes 1048608 | tf_op jit(solution)/shard_map/all_to_all | solution.py:121
  248.9 2.6 gather_fusion.1
  251.5 1.4 reshape.152
  252.8 0.7 multiply_reduce_fusion
  253.6 1.9 fusion.28
  (87 shorter events, 1.7 us)
Async XLA Ops:
  6.5 22.2 %copy-start = (bf16[256,2048]{1,0:T(8,128)(2,1)S(1)}, bf16[256,2048]{1,0:T(8,128)(2,1)}, u32[]{:S(2)}) copy-start(bf16[256,2048]{1,0:T(8,128)(2,1)} %param.26) | copy-start | bytes 3145732
  6.5 60.7 %copy-start.1 = (bf16[128,2048]{1,0:T(8,128)(2,1)S(1)}, bf16[128,2048]{1,0:T(8,128)(2,1)}, u32[]{:S(2)}) copy-start(bf16[128,2048]{1,0:T(8,128)(2,1)} %param.19) | copy-start | bytes 1572868
  6.5 60.6 %all-reduce.3.cloned.1.call-start = ((), (), s32[]{:S(2)}) async-start(), calls=%async_computation.2 | async-start | bytes 2097152 | tf_op jit(solution)/shard_map/psum | solution.py:65
  7.6 11.5 %collective-permute-start = (bf16[30,256]{1,0:T(8,128)(2,1)S(1)}, bf16[30,256]{1,0:T(8,128)(2,1)S(1)}, u32[]{:S(2)}, u32[]{:S(2)}) collective-permute-start(bf16[30,256]{1,0:T(8,128)(2,1)S(1)} %slice.16), channel_id=1, source_target_pairs={{0,4},{4,8},{8,12},{12,16},{16,20},{20,24},{24,28},{1,5},{5,9},{9,... | collective-permute-start | bytes 46088 | tf_op jit(solution)/shard_map/ppermute | solution.py:13
  14.2 54.5 %copy-start.2 = (f32[2048]{0:T(1024)S(1)}, f32[2048]{0:T(1024)}, u32[]{:S(2)}) copy-start(f32[2048]{0:T(1024)} %param.27) | copy-start | bytes 24580
  30.9 103.7 %all-gather.3.cloned.1.call-start = ((), (), s32[]{:S(2)}) async-start(), calls=%async_computation.3 | async-start | bytes 5242880 | tf_op jit(solution)/shard_map/all_gather | solution.py:109
  101.1 106.0 %all-gather.5.cloned.1.call-start = ((), (), s32[]{:S(2)}) async-start(), calls=%async_computation.4 | async-start | bytes 10485760 | tf_op jit(solution)/shard_map/all_gather | solution.py:116
  134.5 7.7 %copy-start.4 = (bf16[1,2048,1024]{2,1,0:T(8,128)(2,1)S(1)}, bf16[1,2048,1024]{2,1,0:T(8,128)(2,1)}, u32[]{:S(2)}) copy-start(bf16[1,2048,1024]{2,1,0:T(8,128)(2,1)} %param.30) | copy-start | bytes 12582916
  134.5 7.7 %copy-start.5 = (bf16[8,1,128,2048]{3,2,0,1:T(8,128)(2,1)S(1)}, bf16[8,1,128,2048]{3,2,0,1:T(8,128)(2,1)}, u32[]{:S(2)}) copy-start(bf16[8,1,128,2048]{3,2,0,1:T(8,128)(2,1)} %all-gather.3.cloned.1.call-done) | copy-start | bytes 12582916
  148.6 74.0 %copy-start.3 = (f32[128,4]{0,1:T(4,128)S(1)}, f32[128,4]{0,1:T(4,128)}, u32[]{:S(2)}) copy-start(f32[128,4]{0,1:T(4,128)} %param.29) | copy-start | bytes 6148
  217.2 31.7 %all-to-all-start.1 = ((bf16[8,1,128,512]{3,2,1,0:T(8,128)(2,1)}), bf16[8,1,128,512]{3,2,1,0:T(8,128)(2,1)S(1)}, u32[]{:S(2)}, u32[]{:S(2)}) async-start(bf16[8,1,128,512]{3,2,1,0:T(8,128)(2,1)} %fusion.22), calls=%async_computation.1 | async-start | bytes 2097152 | tf_op jit(solution)/shard_map/all_to_all | solution.py:121
Sparse Core Ops, SparseCore 0:
  31.0 36.1 all-reduce.2
  101.2 33.3 all-gather.2
  148.7 58.2 all-gather.4
where the time goes:
time: 263 us; the launch traced here: 262 us
  waiting for transfers between devices  146 us (56%)
  blocking collectives  42.4 us (16%)
  matrix products  30.9 us (12%)
  between operations  13.3 us (5%)
  starting transfers between devices  10.5 us (4%)
  local copies, waits for them, and re-layouts  10.4 us (4%)
  other arithmetic  7.78 us (3%)
    all_gather x1, waiting for transfers between devices, body(): lax.all_gather(expert_hidden, 'tp', axis=3, tiled=True)  58.4 us
    psum x1, waiting for transfers between devices, body(): projected = lax.psum(partial_proj, 'tp')  36 us
    all_gather x1, waiting for transfers between devices, body(): arrived = lax.all_gather(landed, 'tp', axis=2, tiled=True)  33.4 us
    all_to_all x1, blocking collectives, body(): lax.all_to_all(jnp.where((own_owners > 0)[..., None], taken, jnp.zeros(()...  30.6 us
    all_to_all x1, waiting for transfers between devices, body(): lax.all_to_all(expert_out, 'sp', split_axis=0, concat_axis=0, tiled=True)  17.9 us
    dot_general x1, matrix products, body(): jnp.einsum('sxcf,xfd->sxcd', lax.all_gather(expert_hidden, 'tp', axis=3,...  10.1 us
    dot_general x1, matrix products, body(): jnp.einsum('sxcd,xdf->sxcf', arrived, exp_up, preferred_element_type=jnp....  7.65 us
    dot_general x1, matrix products, body(): jnp.einsum('sxcd,xdf->sxcf', arrived, exp_gate, preferred_element_type=jn...  6.37 us
  transfers between devices with their start and end apart: 5, of which 4 were waited for; matrix products, arithmetic and copies ran while one was open for 4% of the time, Pallas kernels for 0%

commit v1 on v0

--- a/solution.py
+++ b/solution.py
@@ -111,12 +111,21 @@
     up_part = jnp.einsum("sxcd,xdf->sxcf", arrived, exp_up, preferred_element_type=jnp.float32)
     expert_hidden = (jax.nn.silu(gate_part) * up_part).astype(jnp.bfloat16)
     weight_rows = exp_down
-    expert_sum = jnp.einsum(
-        "sxcf,xfd->sxcd",
-        lax.all_gather(expert_hidden, "tp", axis=3, tiled=True),
-        weight_rows,
-        preferred_element_type=jnp.float32,
-    )
+    count, index, width = (lax.axis_size("tp"), lax.axis_index("tp"), expert_hidden.shape[3])
+    right = [(i_2, (i_2 + 1) % count) for i_2 in range(count)]
+    held, expert_sum = (expert_hidden, None)
+    for step in range(count):
+        coming = lax.ppermute(held, "tp", right) if step < count - 1 else None
+        absorb = jnp.einsum(
+            "sxcf,xfd->sxcd",
+            held,
+            lax.dynamic_slice_in_dim(
+                weight_rows, (index - step) % count * width, held.shape[3], axis=1
+            ),
+            preferred_element_type=jnp.float32,
+        )
+        expert_sum = absorb if expert_sum is None else expert_sum + absorb
+        held = coming
     expert_out = expert_sum.astype(jnp.bfloat16)
     returned = lax.all_to_all(expert_out, "sp", split_axis=0, concat_axis=0, tiled=True)
     flat_out = returned.reshape(experts_all * capacity, col_width)

time: 263 us -> 275 us (1.046)
  waiting for transfers between devices: 146 us -> 155 us
  local copies, waits for them, and re-layouts: 10.4 us -> 13.2 us
    ppermute x0 -> x3, waiting for transfers between devices: none -> 68.5 us  [body(): coming = lax.ppermute(held, 'tp', right) if step < count - 1 else None]
    all_gather x1 -> x0, waiting for transfers between devices: 58.4 us -> none  [body(): lax.all_gather(expert_hidden, 'tp', axis=3, tiled=True)]
    unnamed x14 -> x28, local copies, waits for them, and re-layouts: 0.93 us -> 4.88 us
    dot_general x1 -> x4, matrix products: 10.1 us -> 11.5 us  [body(): jnp.einsum('sxcf,xfd->sxcd', held, lax.dynamic_slice_in_dim(weight_rows,...]
  transfers between devices with their start and end apart: 5 -> 7, of which waited for: 4 -> 6; matrix products, arithmetic and copies ran while one was open for 4% -> 6% of each run, Pallas kernels for 0% -> 0%
where the time goes in v1:
time: 275 us; the launch traced here: 274 us
  waiting for transfers between devices  155 us (56%)
  blocking collectives  42.4 us (15%)
  matrix products  30.1 us (11%)
  between operations  13.7 us (5%)
  local copies, waits for them, and re-layouts  13.2 us (5%)
  starting transfers between devices  10.7 us (4%)
  other arithmetic  7.79 us (3%)
    ppermute x3, waiting for transfers between devices, body(): coming = lax.ppermute(held, 'tp', right) if step < count - 1 else None  68.5 us
    psum x1, waiting for transfers between devices, body(): projected = lax.psum(partial_proj, 'tp')  36 us
    all_gather x1, waiting for transfers between devices, body(): arrived = lax.all_gather(landed, 'tp', axis=2, tiled=True)  33.5 us
    all_to_all x1, blocking collectives, body(): lax.all_to_all(jnp.where((own_owners > 0)[..., None], taken, jnp.zeros(()...  30.6 us
    all_to_all x1, waiting for transfers between devices, body(): lax.all_to_all(expert_out, 'sp', split_axis=0, concat_axis=0, tiled=True)  17.1 us
    dot_general x4, matrix products, body(): jnp.einsum('sxcf,xfd->sxcd', held, lax.dynamic_slice_in_dim(weight_rows,...  11.5 us
    dot_general x1, matrix products, body(): jnp.einsum('sxcd,xdf->sxcf', arrived, exp_up, preferred_element_type=jnp....  7.64 us
    psum x1, blocking collectives, body(): lax.psum((jnp.sum(conv_out, axis=1), jnp.sum(conv_out * conv_out, axis=1)...  6.33 us
  transfers between devices with their start and end apart: 7, of which 6 were waited for; matrix products, arithmetic and copies ran while one was open for 6% of the time, Pallas kernels for 0%

profile of v1, /device:TPU:0, one launch (start us, length us, event | category | flops | bytes accessed | tf_op | source)
XLA Modules:
  0.0 273.9 jit_solution(17125835515036135828)
XLA Ops:
  6.5 1.0 multiply_convert_fusion.1
  7.6 4.9 %collective-permute-start = (bf16[30,256]{1,0:T(8,128)(2,1)S(1)}, bf16[30,256]{1,0:T(8,128)(2,1)S(1)}, u32[]{:S(2)}, u32[]{:S(2)}) collective-permute-start(bf16[30,256]{1,0:T(8,128)(2,1)S(1)} %slice.16), channel_id=1, source_target_pairs={{0,4},{4,8},{8,12},{12,16},{16,20},{20,24},{24,28},{1,5},{5,9},{9,... | collective-permute-start | bytes 46088 | tf_op jit(solution)/shard_map/ppermute | solution.py:13
  12.5 0.7 broadcast_multiply_fusion
  13.2 0.8 copy.34
  14.1 0.1 eq.30
  14.2 0.1 copy.33
  14.3 0.1 mul.150
  14.4 1.1 reduce-window.6
  15.6 0.2 slice_reduce_fusion
  15.9 0.7 convert_element_type.61
  16.7 2.4 scatter_custom_fusion
  19.1 0.7 broadcast_in_dim.14
  19.8 2.4 while.13
  22.3 0.1 fusion.58
  22.4 6.3 %all-reduce = (f32[128]{0:T(128)S(1)}, f32[128]{0:T(128)S(1)}) all-reduce(f32[128]{0:T(128)S(1)} %get-tuple-element.86, f32[128]{0:T(128)S(1)} %get-tuple-element.85), channel_id=1, replica_groups=mesh['sp'=8,'tp'=4] {'tp'}, use_global_device_ids=true, to_apply=%region_5.0 | all-reduce | flops 256 | bytes 2048 | tf_op jit(solution)/shard_map/psum | solution.py:57
  28.7 2.1 fusion.41
  31.2 36.0 %all-reduce.3.cloned.1.call-done = f32[128,2048]{1,0:T(8,128)} async-done(((f32[128,2048]{1,0:T(8,128)}), f32[128,2048]{1,0:T(8,128)}) %all-reduce.3.cloned.1.call-update) | async-done | bytes 1048592 | tf_op jit(solution)/shard_map/psum | solution.py:65
  67.2 1.5 fusion.30
  68.7 0.8 copy-done.1
  69.5 0.2 fusion.32
  69.7 1.4 gather_fusion
  71.1 0.1 broadcast_select_fusion
  71.2 30.6 %all_to_all.10 = bf16[8,1,32,2048]{3,2,1,0:T(8,128)(2,1)} all-to-all(bf16[8,1,32,2048]{3,2,1,0:T(8,128)(2,1)S(1)} %broadcast_select_fusion), channel_id=1, replica_groups=mesh['sp'=8,'tp'=4] {'sp'}, dimensions={0} | all-to-all | bytes 2097152 | tf_op jit(solution)/shard_map/all_to_all | solution.py:102
  101.9 33.5 %all-gather.2.cloned.1.call-done = bf16[8,1,128,2048]{3,2,0,1:T(8,128)(2,1)} async-done(((bf16[8,1,32,2048]{3,2,0,1:T(8,128)(2,1)}), bf16[8,1,128,2048]{3,2,0,1:T(8,128)(2,1)}) %all-gather.2.cloned.1.call-update) | async-done | bytes 4194320 | tf_op jit(solution)/shard_map/all_gather | solution.py:109
  135.4 7.6 %fusion.1 = f32[8,128,1024]{2,1,0:T(8,128)S(1)} fusion(bf16[1,2048,1024]{2,1,0:T(8,128)(2,1)} %param.31, bf16[8,1,128,2048]{3,2,0,1:T(8,128)(2,1)} %all-gather.2.cloned.1.call-done), kind=kOutput, calls=%fused_computation.7 | convolution fusion | flops 4294967296 | bytes 12582912 | tf_op jit(solution)/shard_map/sxcd,xdf->sxcf/dot_general | solution.py:111
  143.1 5.4 %fusion = bf16[8,1,128,1024]{3,2,0,1:T(8,128)(2,1)S(1)} fusion(f32[8,128,1024]{2,1,0:T(8,128)S(1)} %fusion.1, bf16[1,2048,1024]{2,1,0:T(8,128)(2,1)S(1)} %copy-done.7, bf16[8,1,128,2048]{3,2,0,1:T(8,128)(2,1)S(1)} %copy-done.9), kind=kOutput, calls=%fused_computation.6 | convolution fusion | flops 4301258752 | bytes 14680064 | tf_op jit(solution)/shard_map/sxcd,xdf->sxcf/dot_general | solution.py:110
  148.4 1.3 copy-done.10
  149.7 0.2 collective-permute-start.1
  150.0 25.2 %collective-permute-done.1 = bf16[8,1,128,1024]{3,2,0,1:T(8,128)(2,1)S(1)} collective-permute-done((bf16[8,1,128,1024]{3,2,0,1:T(8,128)(2,1)S(1)}, bf16[8,1,128,1024]{3,2,0,1:T(8,128)(2,1)S(1)}, u32[]{:S(2)}, u32[]{:S(2)}) %collective-permute-start.1) | collective-permute-done | bytes 2097184 | tf_op jit(solution)/shard_map/ppermute | solution.py:118
  175.2 1.3 copy-done.11
  176.6 25.6 %collective-permute-done.2 = bf16[8,1,128,1024]{3,2,0,1:T(8,128)(2,1)} collective-permute-done((bf16[8,1,128,1024]{3,2,0,1:T(8,128)(2,1)S(1)}, bf16[8,1,128,1024]{3,2,0,1:T(8,128)(2,1)}, u32[]{:S(2)}, u32[]{:S(2)}) %collective-permute-start.2) | collective-permute-done | bytes 2097184 | tf_op jit(solution)/shard_map/ppermute | solution.py:118
  202.1 3.4 %fusion.20 = f32[512,8,128]{2,0,1:T(8,128)S(1)} fusion(bf16[8,1,128,1024]{3,2,0,1:T(8,128)(2,1)} %copy-done.10, bf16[1,4096,512]{2,1,0:T(8,128)(2,1)} %param.32, s32[]{:T(128)S(6)} %select_n.87), kind=kOutput, calls=%fused_computation.24 | convolution fusion | flops 1073741824 | bytes 5242884 | tf_op jit(solution)/shard_map/sxcf,xfd->sxcd/dot_general | solution.py:119
  205.5 0.4 copy-done.12
  205.9 1.3 fusion.18
  207.2 2.9 %fusion.16 = f32[512,8,128]{2,0,1:T(8,128)S(1)} fusion(bf16[8,1,128,1024]{3,2,0,1:T(8,128)(2,1)} %collective-permute-done.2, bf16[1,4096,512]{2,1,0:T(8,128)(2,1)S(1)} %copy-done.8, s32[]{:T(128)S(6)} %select_n.96), kind=kOutput, calls=%fused_computation.20 | convolution fusion | flops 1073741824 | bytes 5242884 | tf_op jit(solution)/shard_map/sxcf,xfd->sxcd/dot_general | solution.py:119
  210.2 17.7 %collective-permute-done.3 = bf16[8,1,128,1024]{3,2,0,1:T(8,128)(2,1)} collective-permute-done((bf16[8,1,128,1024]{3,2,0,1:T(8,128)(2,1)}, bf16[8,1,128,1024]{3,2,0,1:T(8,128)(2,1)}, u32[]{:S(2)}, u32[]{:S(2)}) %collective-permute-start.3) | collective-permute-done | bytes 2097184 | tf_op jit(solution)/shard_map/ppermute | solution.py:118
  227.9 4.0 %fusion.24 = bf16[8,1,128,512]{2,3,1,0:T(8,128)(2,1)} fusion(bf16[8,1,128,1024]{3,2,0,1:T(8,128)(2,1)} %collective-permute-done.3, f32[512,8,128]{2,0,1:T(8,128)S(1)} %fusion.16, f32[512,8,128]{2,0,1:T(8,128)S(1)} %fusion.20, f32[512,8,128]{2,0,1:T(8,128)S(1)} %fusion.18, bf16[1,4096,512]{2,1,0:T(8,128)(2,1)S(1)} %copy-done.8, s32[]{:T(128)S(6)} %select_n.98), kind=kOutput, calls=%fused_computation.27 | convolution fusion | flops 1075838976 | bytes 10485764 | tf_op jit(solution)/shard_map/sxcf,xfd->sxcd/dot_general | solution.py:119
  231.9 5.5 %all-to-all-start.1 = ((bf16[8,1,128,512]{2,3,1,0:T(8,128)(2,1)}), bf16[8,1,128,512]{2,3,1,0:T(8,128)(2,1)S(1)}, u32[]{:S(2)}, u32[]{:S(2)}) async-start(bf16[8,1,128,512]{2,3,1,0:T(8,128)(2,1)} %fusion.24), calls=%async_computation.1 | async-start | bytes 2097152 | tf_op jit(solution)/shard_map/all_to_all | solution.py:130
  237.4 0.1 copy.43
  237.5 0.3 fusion.59
  237.8 1.3 fusion.29
  239.2 5.4 %all_gather.6 = bf16[128,512]{1,0:T(8,128)(2,1)S(1)} all-gather(bf16[128,128]{1,0:T(8,128)(2,1)S(1)} %fusion.29), channel_id=1, replica_groups=mesh['sp'=8,'tp'=4] {'tp'}, dimensions={1}, use_global_device_ids=true | all-gather | bytes 163840 | tf_op jit(solution)/shard_map/all_gather | solution.py:76
  244.6 17.1 %all-to-all-done.1 = bf16[8,1,128,512]{2,3,1,0:T(8,128)(2,1)S(1)} async-done(((bf16[8,1,128,512]{2,3,1,0:T(8,128)(2,1)}), bf16[8,1,128,512]{2,3,1,0:T(8,128)(2,1)S(1)}, u32[]{:S(2)}, u32[]{:S(2)}) %all-to-all-start.1) | async-done | bytes 1048608 | tf_op jit(solution)/shard_map/all_to_all | solution.py:130
  261.7 0.5 copy.42
  262.3 2.0 gather_fusion.1
  264.2 0.3 reshape.182
  264.6 0.7 multiply_reduce_fusion
  265.3 1.8 fusion.28
  (108 shorter events, 2.2 us)
Async XLA Ops:
  6.5 22.2 %copy-start = (bf16[256,2048]{1,0:T(8,128)(2,1)S(1)}, bf16[256,2048]{1,0:T(8,128)(2,1)}, u32[]{:S(2)}) copy-start(bf16[256,2048]{1,0:T(8,128)(2,1)} %param.26) | copy-start | bytes 3145732
  6.5 60.7 %copy-start.2 = (bf16[128,2048]{1,0:T(8,128)(2,1)S(1)}, bf16[128,2048]{1,0:T(8,128)(2,1)}, u32[]{:S(2)}) copy-start(bf16[128,2048]{1,0:T(8,128)(2,1)} %param.19) | copy-start | bytes 1572868
  6.5 60.7 %all-reduce.3.cloned.1.call-start = ((), (), s32[]{:S(2)}) async-start(), calls=%async_computation.2 | async-start | bytes 2097152 | tf_op jit(solution)/shard_map/psum | solution.py:65
  7.6 11.5 %collective-permute-start = (bf16[30,256]{1,0:T(8,128)(2,1)S(1)}, bf16[30,256]{1,0:T(8,128)(2,1)S(1)}, u32[]{:S(2)}, u32[]{:S(2)}) collective-permute-start(bf16[30,256]{1,0:T(8,128)(2,1)S(1)} %slice.16), channel_id=1, source_target_pairs={{0,4},{4,8},{8,12},{12,16},{16,20},{20,24},{24,28},{1,5},{5,9},{9,... | collective-permute-start | bytes 46088 | tf_op jit(solution)/shard_map/ppermute | solution.py:13
  14.2 55.3 %copy-start.5 = (f32[2048]{0:T(1024)S(1)}, f32[2048]{0:T(1024)}, u32[]{:S(2)}) copy-start(f32[2048]{0:T(1024)} %param.27) | copy-start | bytes 24580
  30.9 104.5 %all-gather.2.cloned.1.call-start = ((), (), s32[]{:S(2)}) async-start(), calls=%async_computation.3 | async-start | bytes 5242880 | tf_op jit(solution)/shard_map/all_gather | solution.py:109
  68.7 0.8 copy-start.1
  135.4 7.7 %copy-start.7 = (bf16[1,2048,1024]{2,1,0:T(8,128)(2,1)S(1)}, bf16[1,2048,1024]{2,1,0:T(8,128)(2,1)}, u32[]{:S(2)}) copy-start(bf16[1,2048,1024]{2,1,0:T(8,128)(2,1)} %param.30) | copy-start | bytes 12582916
  135.4 7.7 %copy-start.9 = (bf16[8,1,128,2048]{3,2,0,1:T(8,128)(2,1)S(1)}, bf16[8,1,128,2048]{3,2,0,1:T(8,128)(2,1)}, u32[]{:S(2)}) copy-start(bf16[8,1,128,2048]{3,2,0,1:T(8,128)(2,1)} %all-gather.2.cloned.1.call-done) | copy-start | bytes 12582916
  148.4 1.3 copy-start.10
  149.7 25.5 %collective-permute-start.1 = (bf16[8,1,128,1024]{3,2,0,1:T(8,128)(2,1)S(1)}, bf16[8,1,128,1024]{3,2,0,1:T(8,128)(2,1)S(1)}, u32[]{:S(2)}, u32[]{:S(2)}) collective-permute-start(bf16[8,1,128,1024]{3,2,0,1:T(8,128)(2,1)S(1)} %fusion), channel_id=1, source_target_pairs={{0,1},{1,2},{2,3},{3,0},{4,5},{5,6},{6,7},{7,4},{8,9},{9,10},{10,1... | collective-permute-start | bytes 6291464 | tf_op jit(solution)/shard_map/ppermute | solution.py:118
  175.2 1.3 copy-start.11
  176.6 25.6 %collective-permute-start.2 = (bf16[8,1,128,1024]{3,2,0,1:T(8,128)(2,1)S(1)}, bf16[8,1,128,1024]{3,2,0,1:T(8,128)(2,1)}, u32[]{:S(2)}, u32[]{:S(2)}) collective-permute-start(bf16[8,1,128,1024]{3,2,0,1:T(8,128)(2,1)S(1)} %collective-permute-done.1), channel_id=1, source_target_pairs={{0,1},{1,2},{2,3},{3,0},{4,5},{5,6},{6,7},{7,4},{8,9},{9,10},{10,1... | collective-permute-start | bytes 6291464 | tf_op jit(solution)/shard_map/ppermute | solution.py:118
  202.1 25.8 %collective-permute-start.3 = (bf16[8,1,128,1024]{3,2,0,1:T(8,128)(2,1)}, bf16[8,1,128,1024]{3,2,0,1:T(8,128)(2,1)}, u32[]{:S(2)}, u32[]{:S(2)}) collective-permute-start(bf16[8,1,128,1024]{3,2,0,1:T(8,128)(2,1)} %collective-permute-done.2), channel_id=1, source_target_pairs={{0,1},{1,2},{2,3},{3,0},{4,5},{5,6},{6,7},{7,4},{8,9},{9,10},{10,1... | collective-permute-start | bytes 6291464 | tf_op jit(solution)/shard_map/ppermute | solution.py:118
  202.1 3.4 %copy-start.8 = (bf16[1,4096,512]{2,1,0:T(8,128)(2,1)S(1)}, bf16[1,4096,512]{2,1,0:T(8,128)(2,1)}, u32[]{:S(2)}) copy-start(bf16[1,4096,512]{2,1,0:T(8,128)(2,1)} %param.32) | copy-start | bytes 12582916
  202.1 3.8 %copy-start.12 = (bf16[8,1,128,1024]{3,2,0,1:T(8,128)(2,1)S(1)}, bf16[8,1,128,1024]{3,2,0,1:T(8,128)(2,1)}, u32[]{:S(2)}) copy-start(bf16[8,1,128,1024]{3,2,0,1:T(8,128)(2,1)} %copy-done.11) | copy-start | bytes 6291460
  210.1 27.3 %copy-start.6 = (f32[128,4]{0,1:T(4,128)S(1)}, f32[128,4]{0,1:T(4,128)}, u32[]{:S(2)}) copy-start(f32[128,4]{0,1:T(4,128)} %param.29) | copy-start | bytes 6148
  210.2 27.4 %copy-start.3 = (bf16[2048,128]{1,0:T(8,128)(2,1)S(1)}, bf16[2048,128]{1,0:T(8,128)(2,1)}, u32[]{:S(2)}) copy-start(bf16[2048,128]{1,0:T(8,128)(2,1)} %param.33) | copy-start | bytes 1572868
  231.9 29.9 %all-to-all-start.1 = ((bf16[8,1,128,512]{2,3,1,0:T(8,128)(2,1)}), bf16[8,1,128,512]{2,3,1,0:T(8,128)(2,1)S(1)}, u32[]{:S(2)}, u32[]{:S(2)}) async-start(bf16[8,1,128,512]{2,3,1,0:T(8,128)(2,1)} %fusion.24), calls=%async_computation.1 | async-start | bytes 2097152 | tf_op jit(solution)/shard_map/all_to_all | solution.py:130
  262.3 3.0 %copy-start.4 = (bf16[512,512]{1,0:T(8,128)(2,1)S(1)}, bf16[512,512]{1,0:T(8,128)(2,1)}, u32[]{:S(2)}) copy-start(bf16[512,512]{1,0:T(8,128)(2,1)} %param.35) | copy-start | bytes 1572868
Sparse Core Ops, SparseCore 0:
  31.0 36.1 all-reduce.2
  102.0 33.3 all-gather.1
